TPU v7x, 32 devices: a whole 2x2x4 slice. The times are simulated.
32 devices in a mesh: dp: 4 (over y, x), kv: 4 (over z), tp: 2 (over core).
Axes of the slice: x: 2, y: 2, z: 4, core: 2. Of those that a mesh axis runs over, the one named last changes fastest.
Arguments:
- tokens: bfloat16 [32, 2048], P('dp', 'kv'), may hold values from -6 to 6
- pre_gain: float32 [2048], P('kv'), may hold values from 0.1 to 1.9
- query_weight: bfloat16 [2048, 1024], P('kv', 'tp'), may hold values from -0.125 to 0.125
- key_weight: bfloat16 [2048, 1024], P('kv', 'tp'), may hold values from -0.125 to 0.125
- value_weight: bfloat16 [2048, 1024], P('kv', 'tp'), may hold values from -0.125 to 0.125
- outgate_weight: bfloat16 [2048, 1024], P('kv', 'tp'), may hold values from -0.125 to 0.125
- input_gate_weight: bfloat16 [2048, 4], replicated, may hold values from -0.125 to 0.125
- forget_gate_weight: bfloat16 [2048, 4], replicated, may hold values from -0.125 to 0.125
- cache_keys: bfloat16 [32, 64, 1024], P(('dp', 'kv'), None, 'tp'), may hold values from -6 to 6
- cache_values: bfloat16 [32, 64, 1024], P(('dp', 'kv'), None, 'tp'), may hold values from -6 to 6
- cache_input: float32 [32, 64, 4], P(('dp', 'kv'), None, 'tp'), may hold values from -6 to 250
- cache_forget: float32 [32, 64, 4], P(('dp', 'kv'), None, 'tp'), may hold values from -0.7 to 0
- lengths: int32 [32], P(('dp', 'kv')), may hold values from 1 to 64, 819 in all
- state_matrix: float32 [32, 4, 256, 256], P(('dp', 'kv'), 'tp'), may hold values from -6 to 6
- state_norm: float32 [32, 4, 256], P(('dp', 'kv'), 'tp'), may hold values from -6 to 6
- state_max: float32 [32, 4], P(('dp', 'kv'), 'tp'), may hold values from -4 to 253
- head_gain: float32 [1024], P('tp'), may hold values from 0.1 to 1.9
- out_weight: bfloat16 [1024, 2048], P('tp', 'kv'), may hold values from -0.375 to 0.375
- mixer_gain: float32 [2048], replicated, may hold values from 0.1 to 1.9
- gate_weight: bfloat16 [2048, 5632], P(None, ('kv', 'tp')), may hold values from -0.125 to 0.125
- up_weight: bfloat16 [2048, 5632], P(None, ('kv', 'tp')), may hold values from -0.125 to 0.125
- down_weight: bfloat16 [5632, 2048], P(('kv', 'tp')), may hold values from -0.21875 to 0.21875
Outputs:
- layer_out: bfloat16 [32, 2048], P('dp', ('kv', 'tp'))
Inputs may be any that keep to these rules, and one draw needn't show every extreme that they name: `lengths`: positions from a sequence's length on take no part.
All inputs are finite; a program needn't handle non-finite values. No bound on the sum of `lengths` on one device may be relied on, other than what follows from the above.
Results may differ from a plain program's by a relative error of at most 0.018.
Values may be sent and summed in bfloat16 or wider, within the bound.
No kernel may reach another device: no remote copies, remote signals or barrier semaphores. Data moves between devices by JAX's collectives and lax.ppermute only.
A program may use at most 64 MiB of HBM per device.

v0:
```python
import jax
import jax.numpy as jnp
from jax import lax
from jax.sharding import PartitionSpec as P

EPS = 1e-06


def per_device(
    tokens,
    pre_gain,
    query_weight,
    key_weight,
    value_weight,
    outgate_weight,
    input_gate_weight,
    forget_gate_weight,
    cache_keys,
    cache_values,
    cache_input,
    cache_forget,
    lengths,
    state_matrix,
    state_norm,
    state_max,
    head_gain,
    out_weight,
    mixer_gain,
    gate_weight,
    up_weight,
    down_weight,
):
    col_width = tokens.shape[1]
    own_seqs = cache_keys.shape[0]
    block_len = cache_keys.shape[1]
    head_count = state_max.shape[1]
    head_size = state_norm.shape[2]
    shard_index = lax.axis_index("kv")
    half_index = lax.axis_index("tp")
    kv_count = lax.axis_size("kv")
    model_width = col_width * kv_count
    token_values = tokens.astype(jnp.float32)
    squares = jnp.sum(token_values * token_values, axis=1)
    normed = (token_values * pre_gain[None, :]).astype(jnp.bfloat16)
    corner = (shard_index * col_width, half_index * head_count)
    gate_pair = jnp.concatenate(
        [
            lax.dynamic_slice(input_gate_weight, corner, (col_width, head_count)),
            lax.dynamic_slice(forget_gate_weight, corner, (col_width, head_count)),
        ],
        axis=1,
    )

    def product(weight):
        return jnp.dot(normed, weight, preferred_element_type=jnp.float32)

    query_term = product(query_weight)
    key_term = product(key_weight)
    value_term = product(value_weight)
    outgate_term = product(outgate_weight)
    gate_term = product(gate_pair)
    square_totals = lax.psum(squares, "kv")
    query_sum, key_sum, value_sum, outgate_sum, gate_sum = (
        lax.psum_scatter(query_term, "kv", scatter_dimension=0, tiled=True),
        lax.psum_scatter(key_term, "kv", scatter_dimension=0, tiled=True),
        lax.psum_scatter(value_term, "kv", scatter_dimension=0, tiled=True),
        lax.psum_scatter(outgate_term, "kv", scatter_dimension=0, tiled=True),
        lax.psum_scatter(gate_term, "kv", scatter_dimension=0, tiled=True),
    )
    own_squares = lax.dynamic_slice_in_dim(square_totals, shard_index * own_seqs, own_seqs, 0)
    scale_first = lax.rsqrt(own_squares / model_width + EPS)[:, None]
    query = (scale_first * query_sum).astype(jnp.bfloat16)
    keys_new = (scale_first * key_sum).astype(jnp.bfloat16)
    values_new = (scale_first * value_sum).astype(jnp.bfloat16)
    outgate = (scale_first * outgate_sum).astype(jnp.bfloat16)
    gate_values = scale_first * gate_sum
    in_gate = gate_values[:, :head_count]
    forget_new = jax.nn.log_sigmoid(gate_values[:, head_count:])
    query_heads = query.reshape(own_seqs, head_count, head_size)
    key_heads = keys_new.reshape(own_seqs, head_count, head_size)
    value_heads = values_new.reshape(own_seqs, head_count, head_size)
    cached_keys = cache_keys.reshape(own_seqs, block_len, head_count, head_size)
    cached_values = cache_values.reshape(own_seqs, block_len, head_count, head_size)
    inv_root = head_size ** (-0.5)
    live_mask = (lax.broadcasted_iota(jnp.int32, (own_seqs, block_len), 1) < lengths[:, None])[
        :, :, None
    ]
    forget_live = jnp.where(live_mask, cache_forget, jnp.float32(0.0))
    running = jnp.cumsum(forget_live, axis=1)
    total_log = running[:, -1, :] + forget_new
    weight_log = jnp.where(live_mask, total_log[:, None, :] - running + cache_input, -jnp.inf)
    state_log = total_log + state_max
    peak_log = jnp.maximum(jnp.maximum(state_log, in_gate), jnp.max(weight_log, axis=1))
    key_dots = (
        jnp.einsum("shd,slhd->slh", query_heads, cached_keys, preferred_element_type=jnp.float32)
        * inv_root
    )
    block_scores = jnp.exp(weight_log - peak_log[:, None, :]) * key_dots
    query_scaled = query_heads.astype(jnp.float32) * inv_root
    self_score = jnp.exp(in_gate - peak_log) * jnp.sum(
        query_scaled * key_heads.astype(jnp.float32), axis=2
    )
    carried = jnp.exp(state_log - peak_log)
    block_weights = block_scores.astype(jnp.bfloat16)
    memory_read = jnp.einsum(
        "shvd,shd->shv", state_matrix, query_scaled, precision=lax.Precision.HIGHEST
    )
    norm_read = jnp.einsum("shd,shd->sh", state_norm, query_scaled, precision=lax.Precision.HIGHEST)
    numerator = (
        carried[:, :, None] * memory_read
        + jnp.einsum(
            "slh,slhd->shd", block_weights, cached_values, preferred_element_type=jnp.float32
        )
        + self_score[:, :, None] * value_heads.astype(jnp.float32)
    )
    denominator = carried * norm_read + jnp.sum(block_scores, axis=1) + self_score
    hidden = numerator / jnp.maximum(jnp.abs(denominator), 1.0)[:, :, None]
    mixed_heads = (
        hidden.reshape(own_seqs, head_count * head_size)
        * head_gain[None, :]
        * jax.nn.sigmoid(outgate.astype(jnp.float32))
    ).astype(jnp.bfloat16)
    mix_terms = jnp.dot(
        lax.all_gather(mixed_heads, "kv", axis=0, tiled=True),
        out_weight,
        preferred_element_type=jnp.float32,
    )
    mix_sum = lax.psum_scatter(
        mix_terms.astype(jnp.bfloat16), "tp", scatter_dimension=1, tiled=True
    ).astype(jnp.float32)
    narrow = mix_sum.shape[1]
    residual = (
        lax.dynamic_slice_in_dim(token_values, half_index * narrow, narrow, 1) + mix_sum
    ).astype(jnp.bfloat16)
    piece_wide = lax.all_gather(residual, ("kv", "tp"), axis=1, tiled=True).astype(jnp.float32)
    normed_piece = (piece_wide * mixer_gain[None, :]).astype(jnp.bfloat16)
    gate_acc = jnp.dot(normed_piece, gate_weight, preferred_element_type=jnp.float32)
    up_acc = jnp.dot(normed_piece, up_weight, preferred_element_type=jnp.float32)
    sum_squares = jnp.sum(piece_wide * piece_wide, axis=1)
    gate_acc, up_acc, sum_squares = (gate_acc, up_acc, sum_squares)
    scale_mid = lax.rsqrt(sum_squares / model_width + EPS)[:, None]
    hidden_units = (jax.nn.silu(scale_mid * gate_acc) * (scale_mid * up_acc)).astype(jnp.bfloat16)
    summed = lax.psum_scatter(
        lax.dot_general(
            down_weight, hidden_units, (((0,), (1,)), ((), ())), preferred_element_type=jnp.float32
        ),
        ("kv", "tp"),
        scatter_dimension=0,
        tiled=True,
    )
    mixer_out = summed.T
    return (residual.astype(jnp.float32) + mixer_out).astype(jnp.bfloat16)


def solution(mesh):
    in_specs = (
        P("dp", "kv"),
        P("kv"),
        P("kv", "tp"),
        P("kv", "tp"),
        P("kv", "tp"),
        P("kv", "tp"),
        P(),
        P(),
        P(("dp", "kv"), None, "tp"),
        P(("dp", "kv"), None, "tp"),
        P(("dp", "kv"), None, "tp"),
        P(("dp", "kv"), None, "tp"),
        P(("dp", "kv")),
        P(("dp", "kv"), "tp", None, None),
        P(("dp", "kv"), "tp", None),
        P(("dp", "kv"), "tp"),
        P("tp"),
        P("tp", "kv"),
        P(),
        P(None, ("kv", "tp")),
        P(None, ("kv", "tp")),
        P(("kv", "tp"), None),
    )
    out_specs = P("dp", ("kv", "tp"))
    return jax.shard_map(
        per_device, mesh=mesh, in_specs=in_specs, out_specs=out_specs, check_vma=False
    )
```

profile of v0, /device:TPU:0, one launch (start us, length us, event | category | flops | bytes accessed | tf_op | source)
XLA Modules:
  0.0 147.6 jit_solution(3637259032463186697)
XLA Ops:
  6.5 0.0 copy-start
  6.5 0.0 copy-start.2
  6.5 0.0 copy-start.1
  6.5 0.0 copy-start.3
  6.5 0.0 all-reduce.8.cloned.1.call-start
  6.6 1.6 %multiply_reduce_fusion = f32[8]{0:T(128)} fusion(bf16[8,512]{1,0:T(8,128)(2,1)} %param.22), kind=kLoop, calls=%fused_computation.22 | loop fusion | flops 12280 | bytes 8224 | tf_op jit(solution)/shard_map/reduce_sum | solution.py:43
  8.2 1.9 %fusion.43 = f32[8,512]{1,0:T(8,128)} fusion(bf16[512,512]{1,0:T(8,128)(2,1)} %param.27, f32[512]{0:T(512)} %param.23, bf16[8,512]{1,0:T(8,128)(2,1)} %param.22), kind=kOutput, calls=%fused_computation.73 | convolution fusion | flops 4206592 | bytes 550912 | tf_op jit(solution)/shard_map/dot_general | solution.py:55
  10.0 1.9 %fusion.44 = f32[8,512]{1,0:T(8,128)} fusion(bf16[512,512]{1,0:T(8,128)(2,1)} %param.26, f32[512]{0:T(512)} %param.23, bf16[8,512]{1,0:T(8,128)(2,1)} %param.22), kind=kOutput, calls=%fused_computation.74 | convolution fusion | flops 4206592 | bytes 550912 | tf_op jit(solution)/shard_map/dot_general | solution.py:55
  11.9 1.9 %fusion.46 = f32[8,512]{1,0:T(8,128)} fusion(bf16[512,512]{1,0:T(8,128)(2,1)} %param.24, f32[512]{0:T(512)} %param.23, bf16[8,512]{1,0:T(8,128)(2,1)} %param.22), kind=kOutput, calls=%fused_computation.76 | convolution fusion | flops 4206592 | bytes 550912 | tf_op jit(solution)/shard_map/dot_general | solution.py:55
  13.7 0.8 dynamic_slice.15
  14.5 0.8 dynamic_slice.14
  15.3 1.9 %fusion.45 = f32[8,512]{1,0:T(8,128)} fusion(bf16[512,512]{1,0:T(8,128)(2,1)} %param.25, f32[512]{0:T(512)} %param.23, bf16[8,512]{1,0:T(8,128)(2,1)} %param.22), kind=kOutput, calls=%fused_computation.75 | convolution fusion | flops 4206592 | bytes 550912 | tf_op jit(solution)/shard_map/dot_general | solution.py:55
  17.1 1.4 fusion.21
  18.5 0.0 all-reduce.8.cloned.1.call-update
  18.6 0.0 reduce-scatter.3.cloned.1.call-start
  18.6 0.7 iota_compare_fusion
  19.3 0.0 copy-start.4
  19.3 0.7 broadcast_select_fusion
  20.0 0.0 copy-done.4
  20.0 0.1 copy.39
  20.1 0.1 reduce_window_sum.11
  20.2 0.1 copy.40
  20.3 1.3 dynamic-slice
  22.3 34.1 %all-reduce.8.cloned.1.call-done = (f32[8,512]{1,0:T(8,128)}, f32[8]{0:T(128)}, f32[8,512]{1,0:T(8,128)}, f32[8,512]{1,0:T(8,128)}, f32[8,4]{1,0:T(8,128)}, /*index=5*/f32[8,512]{1,0:T(8,128)}) async-done(((f32[8,512]{1,0:T(8,128)}, f32[8]{0:T(128)}, f32[8,512]{1,0:T(8,128)}, f32[8,512]{1,0:T(8,128)}, f32[8,4]{1,0:T(8,128)}, /*index=5*/f32[8,512]{1,0:T(8,128)}), (f32[8,512]{1,0:T(8,128)}, f32[8]{0:T(128)}, ...) | async-done | bytes 65712
  56.3 0.7 add_rsqrt_fusion.1
  57.1 0.8 fusion.37
  57.9 0.7 fusion.40
  58.7 1.0 fusion.5
  59.7 0.1 fusion.42
  59.8 0.9 fusion.49
  60.7 0.7 maximum_maximum_fusion
  61.4 0.8 fusion.50
  62.2 1.0 fusion.2
  63.2 0.8 multiply_reduce_fusion.1
  64.0 2.2 %fusion.31 = f32[2,2,1,256]{3,2,1,0:T(1,128)S(1)} fusion(f32[2,2,256,256]{3,2,1,0:T(8,128)} %param.35, f32[2,2,256,1]{2,1,0,3:T(2,128)S(1)} %get-tuple-element.20), kind=kOutput, calls=%fused_computation.46 | convolution fusion | flops 3145728 | bytes 1056768 | tf_op jit(solution)/shard_map/shvd,shd->shv/dot_general | solution.py:105
  66.2 0.1 fusion.35
  66.3 0.8 fusion.39
  67.1 12.0 %all-gather = bf16[4,2,512]{2,1,0:T(2,128)(2,1)S(1)} all-gather(bf16[1,2,512]{2,1,0:T(2,128)(2,1)S(1)} %fusion.39), channel_id=1, replica_groups=mesh['dp'=4,'kv'=4,'tp'=2] {'kv'}, dimensions={0}, use_global_device_ids=true | all-gather | bytes 10240 | tf_op jit(solution)/shard_map/all_gather | solution.py:124
  79.1 0.0 copy-done.1
  79.1 0.8 convolution_convert_fusion
  79.9 0.0 reduce-scatter.3.cloned.1.call-update
  79.9 0.0 reduce-scatter.5.cloned.1.call-start
  80.0 0.0 copy-done.2
  80.0 6.4 %reduce-scatter.3.cloned.1.call-done = bf16[8,256]{1,0:T(8,128)(2,1)} async-done(((bf16[8,512]{1,0:T(8,128)(2,1)}), bf16[8,256]{1,0:T(8,128)(2,1)}) %reduce-scatter.3.cloned.1.call-update) | async-done | bytes 4112 | tf_op jit(solution)/shard_map/reduce_scatter | solution.py:128
  86.3 0.7 add_convert_fusion
  87.0 14.3 %all_gather.7 = bf16[8,2048]{1,0:T(8,128)(2,1)S(1)} all-gather(bf16[8,256]{1,0:T(8,128)(2,1)S(1)} %add_convert_fusion), channel_id=1, replica_groups=mesh['dp'=4,'kv'=4,'tp'=2] {'kv','tp'}, dimensions={1}, use_global_device_ids=true | all-gather | bytes 36864 | tf_op jit(solution)/shard_map/all_gather | solution.py:135
  101.3 0.1 fusion.8
  101.5 0.0 copy-done.3
  101.5 2.7 %convolution_multiply_fusion.1 = f32[8,704]{1,0:T(8,128)S(1)} fusion(bf16[2048,704]{0,1:T(8,128)(2,1)} %param.41, bf16[8,2048]{1,0:T(8,128)(2,1)S(1)} %all_gather.7, f32[2048]{0:T(1024)S(1)} %copy-done.3, f32[8]{0:T(128)S(1)} %add_rsqrt_fusion), kind=kOutput, calls=%fused_computation.3 | convolution fusion | flops 23123456 | bytes 2947104 | tf_op jit(solution)/shard_map/dot_general | solution.py:137
  104.2 0.0 copy-done
  104.2 4.1 %convolution_bitcast_fusion = f32[2048,8]{0,1:T(8,128)} fusion(bf16[704,2048]{1,0:T(8,128)(2,1)S(1)} %copy-done, bf16[2048,704]{0,1:T(8,128)(2,1)} %param.42, bf16[8,2048]{1,0:T(8,128)(2,1)S(1)} %all_gather.7, f32[2048]{0:T(1024)S(1)} %copy-done.3, f32[8,704]{1,0:T(8,128)S(1)} %convolution_multiply_fusion.1, f32[8]{0:T(128)S(1)} %add_rsqrt_fusion), kind=kOutput, calls=%fused_computation | convolution fusion | flops 46225920 | bytes 5896224 | tf_op jit(solution)/shard_map/dot_general | solution.py:144
  108.3 0.0 reduce-scatter.5.cloned.1.call-update
  108.3 31.5 %reduce-scatter.5.cloned.1.call-done = f32[256,8]{0,1:T(8,128)} async-done(((f32[2048,8]{0,1:T(8,128)}), f32[256,8]{0,1:T(8,128)}) %reduce-scatter.5.cloned.1.call-update) | async-done | bytes 8208 | tf_op jit(solution)/shard_map/reduce_scatter | solution.py:143
  139.8 1.3 fusion.20
  (10 shorter events, 0.1 us)
Async XLA Ops:
  6.5 97.6 %copy-start = (bf16[704,2048]{1,0:T(8,128)(2,1)S(1)}, bf16[704,2048]{1,0:T(8,128)(2,1)}, u32[]{:S(2)}) copy-start(bf16[704,2048]{1,0:T(8,128)(2,1)} %param.43) | copy-start | bytes 8650756
  6.5 73.4 %copy-start.2 = (bf16[8,512]{1,0:T(8,128)(2,1)S(1)}, bf16[8,512]{1,0:T(8,128)(2,1)}, u32[]{:S(2)}) copy-start(bf16[8,512]{1,0:T(8,128)(2,1)} %param.22) | copy-start | bytes 24580
  6.5 72.6 %copy-start.1 = (bf16[512,512]{1,0:T(8,128)(2,1)S(1)}, bf16[512,512]{1,0:T(8,128)(2,1)}, u32[]{:S(2)}) copy-start(bf16[512,512]{1,0:T(8,128)(2,1)} %param.39) | copy-start | bytes 1572868
  6.5 94.9 %copy-start.3 = (f32[2048]{0:T(1024)S(1)}, f32[2048]{0:T(1024)}, u32[]{:S(2)}) copy-start(f32[2048]{0:T(1024)} %param.40) | copy-start | bytes 24580
  6.5 49.8 %all-reduce.8.cloned.1.call-start = ((), (), s32[]{:S(2)}) async-start(), calls=%async_computation.4 | async-start | bytes 140288
  18.6 67.8 %reduce-scatter.3.cloned.1.call-start = ((), (), s32[]{:S(2)}) async-start(), calls=%async_computation.2 | async-start | bytes 12288 | tf_op jit(solution)/shard_map/reduce_scatter | solution.py:128
  19.3 0.7 copy-start.4
  79.9 59.9 %reduce-scatter.5.cloned.1.call-start = ((), (), s32[]{:S(2)}) async-start(), calls=%async_computation.3 | async-start | bytes 73728 | tf_op jit(solution)/shard_map/reduce_scatter | solution.py:143
Sparse Core Ops, SparseCore 0:
  18.7 37.6 all-reduce.7
  80.0 6.2 reduce-scatter.2
  108.4 31.2 reduce-scatter.4
where the time goes:
time: 149 us; the launch traced here: 148 us
  waiting for transfers between devices  71.9 us (48%)
  blocking collectives  26.3 us (18%)
  matrix products  20.6 us (14%)
  between operations  13.8 us (9%)
  other arithmetic  11.7 us (8%)
  local copies, waits for them, and re-layouts  3.11 us (2%)
    unnamed x4, waiting for transfers between devices  34.1 us
    reduce_scatter x1, waiting for transfers between devices, per_device(): lax.psum_scatter(lax.dot_general(down_weight, hidden_units, (((0,), (1,))...  31.5 us
    all_gather x1, blocking collectives, per_device(): lax.all_gather(residual, ('kv', 'tp'), axis=1, tiled=True)  14.3 us
    all_gather x1, blocking collectives, per_device(): lax.all_gather(mixed_heads, 'kv', axis=0, tiled=True)  12 us
    dot_general x5, matrix products, product(): return jnp.dot(normed, weight, preferred_element_type=jnp.float32)  8.84 us
    reduce_scatter x1, waiting for transfers between devices, per_device(): lax.psum_scatter(mix_terms.astype(jnp.bfloat16), 'tp', scatter_dimension=...  6.35 us
    dot_general x1, matrix products, per_device(): lax.dot_general(down_weight, hidden_units, (((0,), (1,)), ((), ())), pref...  4.12 us
  transfers between devices with their start and end apart: 3, of which 3 were waited for; matrix products, arithmetic and copies ran while one was open for 2% of the time, Pallas kernels for 0%

commit v1 on v0

--- a/solution.py
+++ b/solution.py
@@ -4,6 +4,18 @@
 from jax.sharding import PartitionSpec as P
 
 EPS = 1e-06
+
+
+def ring_gather(array, axis, dim):
+    ways, here, hop = (lax.axis_size(axis), lax.axis_index(axis), array.shape[dim])
+    shape = [n * ways if d == dim else n for d, n in enumerate(array.shape)]
+    full = lax.dynamic_update_slice_in_dim(
+        jnp.zeros(shape, array.dtype), array, here * hop, axis=dim
+    )
+    for far in range(1, ways):
+        array = lax.ppermute(array, axis, [(d, (d + 1) % ways) for d in range(ways)])
+        full = lax.dynamic_update_slice_in_dim(full, array, (here - far) % ways * hop, axis=dim)
+    return full
 
 
 def per_device(
@@ -132,7 +144,7 @@
     residual = (
         lax.dynamic_slice_in_dim(token_values, half_index * narrow, narrow, 1) + mix_sum
     ).astype(jnp.bfloat16)
-    piece_wide = lax.all_gather(residual, ("kv", "tp"), axis=1, tiled=True).astype(jnp.float32)
+    piece_wide = ring_gather(residual, ("kv", "tp"), 1).astype(jnp.float32)
     normed_piece = (piece_wide * mixer_gain[None, :]).astype(jnp.bfloat16)
     gate_acc = jnp.dot(normed_piece, gate_weight, preferred_element_type=jnp.float32)
     up_acc = jnp.dot(normed_piece, up_weight, preferred_element_type=jnp.float32)

time: 149 us -> 166 us (1.11)
  waiting for transfers between devices: 71.9 us -> 103 us
  blocking collectives: 26.3 us -> 12 us
    ppermute x0 -> x7, waiting for transfers between devices: none -> 33.6 us  [ring_gather(): lax.ppermute(array, axis, [(d, (d + 1) % ways) for d in range(ways)])]
    all_gather x1 -> x0, blocking collectives: 14.3 us -> none  [per_device(): lax.all_gather(residual, ('kv', 'tp'), axis=1, tiled=True)]
    reduce_scatter x1, waiting for transfers between devices: 31.5 us -> 29 us  [per_device(): lax.psum_scatter(lax.dot_general(down_weight, hidden_units, (((0,), (1,))...]
  transfers between devices with their start and end apart: 3 -> 10, of which waited for: 3 -> 10; matrix products, arithmetic and copies ran while one was open for 2% -> 2% of each run, Pallas kernels for 0% -> 0%
where the time goes in v1:
time: 166 us; the launch traced here: 165 us
  waiting for transfers between devices  103 us (62%)
  matrix products  20.6 us (12%)
  between operations  13.9 us (8%)
  blocking collectives  12 us (7%)
  other arithmetic  11.7 us (7%)
  local copies, waits for them, and re-layouts  3.13 us (2%)
    unnamed x4, waiting for transfers between devices  34.1 us
    ppermute x7, waiting for transfers between devices, ring_gather(): lax.ppermute(array, axis, [(d, (d + 1) % ways) for d in range(ways)])  33.6 us
    reduce_scatter x1, waiting for transfers between devices, per_device(): lax.psum_scatter(lax.dot_general(down_weight, hidden_units, (((0,), (1,))...  29 us
    all_gather x1, blocking collectives, per_device(): lax.all_gather(mixed_heads, 'kv', axis=0, tiled=True)  12 us
    dot_general x5, matrix products, product(): return jnp.dot(normed, weight, preferred_element_type=jnp.float32)  8.84 us
    reduce_scatter x1, waiting for transfers between devices, per_device(): lax.psum_scatter(mix_terms.astype(jnp.bfloat16), 'tp', scatter_dimension=...  6.3 us
    dot_general x1, matrix products, per_device(): lax.dot_general(down_weight, hidden_units, (((0,), (1,)), ((), ())), pref...  4.12 us
  transfers between devices with their start and end apart: 10, of which 10 were waited for; matrix products, arithmetic and copies ran while one was open for 2% of the time, Pallas kernels for 0%

profile of v1, /device:TPU:0, one launch (start us, length us, event | category | flops | bytes accessed | tf_op | source)
XLA Modules:
  0.0 164.6 jit_solution(7517385458960251174)
XLA Ops:
  6.5 0.0 copy-start
  6.5 0.0 copy-start.2
  6.5 0.0 all-reduce.8.cloned.1.call-start
  6.6 1.6 multiply_reduce_fusion
  8.2 1.9 %fusion.43 = f32[8,512]{1,0:T(8,128)} fusion(bf16[512,512]{1,0:T(8,128)(2,1)} %param.27, f32[512]{0:T(512)} %param.23, bf16[8,512]{1,0:T(8,128)(2,1)} %param.22), kind=kOutput, calls=%fused_computation.81 | convolution fusion | flops 4206592 | bytes 550912 | tf_op jit(solution)/shard_map/dot_general | solution.py:67
  10.0 1.9 %fusion.44 = f32[8,512]{1,0:T(8,128)} fusion(bf16[512,512]{1,0:T(8,128)(2,1)} %param.26, f32[512]{0:T(512)} %param.23, bf16[8,512]{1,0:T(8,128)(2,1)} %param.22), kind=kOutput, calls=%fused_computation.82 | convolution fusion | flops 4206592 | bytes 550912 | tf_op jit(solution)/shard_map/dot_general | solution.py:67
  11.9 1.9 %fusion.46 = f32[8,512]{1,0:T(8,128)} fusion(bf16[512,512]{1,0:T(8,128)(2,1)} %param.24, f32[512]{0:T(512)} %param.23, bf16[8,512]{1,0:T(8,128)(2,1)} %param.22), kind=kOutput, calls=%fused_computation.84 | convolution fusion | flops 4206592 | bytes 550912 | tf_op jit(solution)/shard_map/dot_general | solution.py:67
  13.7 0.8 dynamic_slice.15
  14.5 0.8 dynamic_slice.14
  15.3 1.9 %fusion.45 = f32[8,512]{1,0:T(8,128)} fusion(bf16[512,512]{1,0:T(8,128)(2,1)} %param.25, f32[512]{0:T(512)} %param.23, bf16[8,512]{1,0:T(8,128)(2,1)} %param.22), kind=kOutput, calls=%fused_computation.83 | convolution fusion | flops 4206592 | bytes 550912 | tf_op jit(solution)/shard_map/dot_general | solution.py:67
  17.1 1.4 fusion.21
  18.5 0.0 all-reduce.8.cloned.1.call-update
  18.6 0.0 reduce-scatter.3.cloned.1.call-start
  18.6 0.7 iota_compare_fusion
  19.3 0.7 broadcast_select_fusion
  20.0 0.0 copy-done.4
  20.0 0.1 copy.39
  20.1 0.1 reduce_window_sum.11
  20.2 0.1 copy.40
  20.3 1.3 dynamic-slice
  22.3 34.1 %all-reduce.8.cloned.1.call-done = (f32[8,512]{1,0:T(8,128)}, f32[8]{0:T(128)}, f32[8,512]{1,0:T(8,128)}, f32[8,512]{1,0:T(8,128)}, f32[8,4]{1,0:T(8,128)}, /*index=5*/f32[8,512]{1,0:T(8,128)}) async-done(((f32[8,512]{1,0:T(8,128)}, f32[8]{0:T(128)}, f32[8,512]{1,0:T(8,128)}, f32[8,512]{1,0:T(8,128)}, f32[8,4]{1,0:T(8,128)}, /*index=5*/f32[8,512]{1,0:T(8,128)}), (f32[8,512]{1,0:T(8,128)}, f32[8]{0:T(128)}, ...) | async-done | bytes 65712
  56.3 0.7 add_rsqrt_fusion.1
  57.1 0.8 fusion.37
  57.9 0.7 fusion.40
  58.7 1.0 fusion.5
  59.7 0.1 fusion.42
  59.8 0.9 fusion.49
  60.7 0.7 maximum_maximum_fusion
  61.4 0.8 fusion.50
  62.2 1.0 fusion.2
  63.2 0.8 multiply_reduce_fusion.1
  64.0 2.2 %fusion.31 = f32[2,2,1,256]{3,2,1,0:T(1,128)S(1)} fusion(f32[2,2,256,256]{3,2,1,0:T(8,128)} %param.35, f32[2,2,256,1]{2,1,0,3:T(2,128)S(1)} %get-tuple-element.22), kind=kOutput, calls=%fused_computation.46 | convolution fusion | flops 3145728 | bytes 1056768 | tf_op jit(solution)/shard_map/shvd,shd->shv/dot_general | solution.py:117
  66.2 0.1 fusion.35
  66.3 0.8 fusion.39
  67.1 12.0 %all-gather = bf16[4,2,512]{2,1,0:T(2,128)(2,1)S(1)} all-gather(bf16[1,2,512]{2,1,0:T(2,128)(2,1)S(1)} %fusion.39), channel_id=1, replica_groups=mesh['dp'=4,'kv'=4,'tp'=2] {'kv'}, dimensions={0}, use_global_device_ids=true | all-gather | bytes 10240 | tf_op jit(solution)/shard_map/all_gather | solution.py:136
  79.1 0.0 copy-done.1
  79.1 0.8 convolution_convert_fusion
  79.9 0.0 reduce-scatter.3.cloned.1.call-update
  79.9 0.0 reduce-scatter.5.cloned.1.call-start
  80.0 0.0 copy-done.2
  80.0 6.3 %reduce-scatter.3.cloned.1.call-done = bf16[8,256]{1,0:T(8,128)(2,1)} async-done(((bf16[8,512]{1,0:T(8,128)(2,1)}), bf16[8,256]{1,0:T(8,128)(2,1)}) %reduce-scatter.3.cloned.1.call-update) | async-done | bytes 4112 | tf_op jit(solution)/shard_map/reduce_scatter | solution.py:140
  86.3 0.7 constant_dynamic-update-slice_fusion.7
  87.0 0.2 collective-permute-start
  87.2 4.6 %collective-permute-done = bf16[8,256]{1,0:T(8,128)(2,1)S(1)} collective-permute-done((bf16[8,256]{1,0:T(8,128)(2,1)S(1)}, bf16[8,256]{1,0:T(8,128)(2,1)S(1)}, u32[]{:S(2)}, u32[]{:S(2)}) %collective-permute-start) | collective-permute-done | bytes 4128 | tf_op jit(solution)/shard_map/ppermute | solution.py:16
  91.8 0.0 collective-permute-start.1
  91.9 4.8 %collective-permute-done.1 = bf16[8,256]{1,0:T(8,128)(2,1)S(1)} collective-permute-done((bf16[8,256]{1,0:T(8,128)(2,1)S(1)}, bf16[8,256]{1,0:T(8,128)(2,1)S(1)}, u32[]{:S(2)}, u32[]{:S(2)}) %collective-permute-start.1) | collective-permute-done | bytes 4128 | tf_op jit(solution)/shard_map/ppermute | solution.py:16
  96.7 0.0 collective-permute-start.2
  96.7 4.8 %collective-permute-done.2 = bf16[8,256]{1,0:T(8,128)(2,1)S(1)} collective-permute-done((bf16[8,256]{1,0:T(8,128)(2,1)S(1)}, bf16[8,256]{1,0:T(8,128)(2,1)S(1)}, u32[]{:S(2)}, u32[]{:S(2)}) %collective-permute-start.2) | collective-permute-done | bytes 4128 | tf_op jit(solution)/shard_map/ppermute | solution.py:16
  101.5 0.0 collective-permute-start.3
  101.5 4.8 %collective-permute-done.3 = bf16[8,256]{1,0:T(8,128)(2,1)S(1)} collective-permute-done((bf16[8,256]{1,0:T(8,128)(2,1)S(1)}, bf16[8,256]{1,0:T(8,128)(2,1)S(1)}, u32[]{:S(2)}, u32[]{:S(2)}) %collective-permute-start.3) | collective-permute-done | bytes 4128 | tf_op jit(solution)/shard_map/ppermute | solution.py:16
  106.3 0.0 collective-permute-start.4
  106.3 4.8 %collective-permute-done.4 = bf16[8,256]{1,0:T(8,128)(2,1)S(1)} collective-permute-done((bf16[8,256]{1,0:T(8,128)(2,1)S(1)}, bf16[8,256]{1,0:T(8,128)(2,1)S(1)}, u32[]{:S(2)}, u32[]{:S(2)}) %collective-permute-start.4) | collective-permute-done | bytes 4128 | tf_op jit(solution)/shard_map/ppermute | solution.py:16
  111.2 0.0 collective-permute-start.5
  111.2 4.8 %collective-permute-done.5 = bf16[8,256]{1,0:T(8,128)(2,1)S(1)} collective-permute-done((bf16[8,256]{1,0:T(8,128)(2,1)S(1)}, bf16[8,256]{1,0:T(8,128)(2,1)S(1)}, u32[]{:S(2)}, u32[]{:S(2)}) %collective-permute-start.5) | collective-permute-done | bytes 4128 | tf_op jit(solution)/shard_map/ppermute | solution.py:16
  116.0 0.0 collective-permute-start.6
  116.0 4.8 %collective-permute-done.6 = bf16[8,256]{1,0:T(8,128)(2,1)S(1)} collective-permute-done((bf16[8,256]{1,0:T(8,128)(2,1)S(1)}, bf16[8,256]{1,0:T(8,128)(2,1)S(1)}, u32[]{:S(2)}, u32[]{:S(2)}) %collective-permute-start.6) | collective-permute-done | bytes 4128 | tf_op jit(solution)/shard_map/ppermute | solution.py:16
  120.8 0.1 fusion.8
  121.0 0.0 copy-done.3
  121.0 2.7 %convolution_multiply_fusion.1 = f32[8,704]{1,0:T(8,128)S(1)} fusion(bf16[2048,704]{0,1:T(8,128)(2,1)} %param.41, bf16[8,2048]{1,0:T(8,128)(2,1)S(1)} %constant_dynamic-update-slice_fusion, f32[2048]{0:T(1024)S(1)} %copy-done.3, f32[8]{0:T(128)S(1)} %add_rsqrt_fusion), kind=kOutput, calls=%fused_computation.3 | convolution fusion | flops 23123456 | bytes 2947104 | tf_op jit(solution)/shard_map/dot_general | solution.py:149
  123.6 0.0 copy-done
  123.6 4.1 %convolution_bitcast_fusion = f32[2048,8]{0,1:T(8,128)} fusion(bf16[704,2048]{1,0:T(8,128)(2,1)S(1)} %copy-done, bf16[2048,704]{0,1:T(8,128)(2,1)} %param.42, bf16[8,2048]{1,0:T(8,128)(2,1)S(1)} %constant_dynamic-update-slice_fusion, f32[2048]{0:T(1024)S(1)} %copy-done.3, f32[8,704]{1,0:T(8,128)S(1)} %convolution_multiply_fusion.1, f32[8]{0:T(128)S(1)} %add_rsqrt_fusion), kind=kOutput, calls=%fused_computation | convolution fusion | flops 46225920 | bytes 5896224 | tf_op jit(solution)/shard_map/dot_general | solution.py:156
  127.8 0.0 reduce-scatter.5.cloned.1.call-update
  127.8 29.0 %reduce-scatter.5.cloned.1.call-done = f32[256,8]{0,1:T(8,128)} async-done(((f32[2048,8]{0,1:T(8,128)}), f32[256,8]{0,1:T(8,128)}) %reduce-scatter.5.cloned.1.call-update) | async-done | bytes 8208 | tf_op jit(solution)/shard_map/reduce_scatter | solution.py:155
  156.8 1.3 fusion.20
  (21 shorter events, 0.1 us)
Async XLA Ops:
  6.5 117.1 %copy-start = (bf16[704,2048]{1,0:T(8,128)(2,1)S(1)}, bf16[704,2048]{1,0:T(8,128)(2,1)}, u32[]{:S(2)}) copy-start(bf16[704,2048]{1,0:T(8,128)(2,1)} %param.43) | copy-start | bytes 8650756
  6.5 73.4 %copy-start.2 = (bf16[8,512]{1,0:T(8,128)(2,1)S(1)}, bf16[8,512]{1,0:T(8,128)(2,1)}, u32[]{:S(2)}) copy-start(bf16[8,512]{1,0:T(8,128)(2,1)} %param.22) | copy-start | bytes 24580
  6.5 72.6 %copy-start.1 = (bf16[512,512]{1,0:T(8,128)(2,1)S(1)}, bf16[512,512]{1,0:T(8,128)(2,1)}, u32[]{:S(2)}) copy-start(bf16[512,512]{1,0:T(8,128)(2,1)} %param.39) | copy-start | bytes 1572868
  6.5 114.4 %copy-start.3 = (f32[2048]{0:T(1024)S(1)}, f32[2048]{0:T(1024)}, u32[]{:S(2)}) copy-start(f32[2048]{0:T(1024)} %param.40) | copy-start | bytes 24580
  6.5 49.8 %all-reduce.8.cloned.1.call-start = ((), (), s32[]{:S(2)}) async-start(), calls=%async_computation.4 | async-start | bytes 140288
  18.6 67.8 %reduce-scatter.3.cloned.1.call-start = ((), (), s32[]{:S(2)}) async-start(), calls=%async_computation.2 | async-start | bytes 12288 | tf_op jit(solution)/shard_map/reduce_scatter | solution.py:140
  19.3 0.7 copy-start.4
  79.9 76.9 %reduce-scatter.5.cloned.1.call-start = ((), (), s32[]{:S(2)}) async-start(), calls=%async_computation.3 | async-start | bytes 73728 | tf_op jit(solution)/shard_map/reduce_scatter | solution.py:155
  87.0 4.8 %collective-permute-start = (bf16[8,256]{1,0:T(8,128)(2,1)S(1)}, bf16[8,256]{1,0:T(8,128)(2,1)S(1)}, u32[]{:S(2)}, u32[]{:S(2)}) collective-permute-start(bf16[8,256]{1,0:T(8,128)(2,1)S(1)} %get-tuple-element.14), channel_id=1, source_target_pairs={{0,1},{1,2},{2,3},{3,4},{4,5},{5,6},{6,7},{7,0},{8,9},{9,10},{10,1... | collective-permute-start | bytes 12296 | tf_op jit(solution)/shard_map/ppermute | solution.py:16
  91.8 4.8 %collective-permute-start.1 = (bf16[8,256]{1,0:T(8,128)(2,1)S(1)}, bf16[8,256]{1,0:T(8,128)(2,1)S(1)}, u32[]{:S(2)}, u32[]{:S(2)}) collective-permute-start(bf16[8,256]{1,0:T(8,128)(2,1)S(1)} %collective-permute-done), channel_id=1, source_target_pairs={{0,1},{1,2},{2,3},{3,4},{4,5},{5,6},{6,7},{7,0},{8,9},{9,10},{10,1... | collective-permute-start | bytes 12296 | tf_op jit(solution)/shard_map/ppermute | solution.py:16
  96.7 4.8 %collective-permute-start.2 = (bf16[8,256]{1,0:T(8,128)(2,1)S(1)}, bf16[8,256]{1,0:T(8,128)(2,1)S(1)}, u32[]{:S(2)}, u32[]{:S(2)}) collective-permute-start(bf16[8,256]{1,0:T(8,128)(2,1)S(1)} %collective-permute-done.1), channel_id=1, source_target_pairs={{0,1},{1,2},{2,3},{3,4},{4,5},{5,6},{6,7},{7,0},{8,9},{9,10},{10,1... | collective-permute-start | bytes 12296 | tf_op jit(solution)/shard_map/ppermute | solution.py:16
  101.5 4.8 %collective-permute-start.3 = (bf16[8,256]{1,0:T(8,128)(2,1)S(1)}, bf16[8,256]{1,0:T(8,128)(2,1)S(1)}, u32[]{:S(2)}, u32[]{:S(2)}) collective-permute-start(bf16[8,256]{1,0:T(8,128)(2,1)S(1)} %collective-permute-done.2), channel_id=1, source_target_pairs={{0,1},{1,2},{2,3},{3,4},{4,5},{5,6},{6,7},{7,0},{8,9},{9,10},{10,1... | collective-permute-start | bytes 12296 | tf_op jit(solution)/shard_map/ppermute | solution.py:16
  106.3 4.8 %collective-permute-start.4 = (bf16[8,256]{1,0:T(8,128)(2,1)S(1)}, bf16[8,256]{1,0:T(8,128)(2,1)S(1)}, u32[]{:S(2)}, u32[]{:S(2)}) collective-permute-start(bf16[8,256]{1,0:T(8,128)(2,1)S(1)} %collective-permute-done.3), channel_id=1, source_target_pairs={{0,1},{1,2},{2,3},{3,4},{4,5},{5,6},{6,7},{7,0},{8,9},{9,10},{10,1... | collective-permute-start | bytes 12296 | tf_op jit(solution)/shard_map/ppermute | solution.py:16
  111.2 4.8 %collective-permute-start.5 = (bf16[8,256]{1,0:T(8,128)(2,1)S(1)}, bf16[8,256]{1,0:T(8,128)(2,1)S(1)}, u32[]{:S(2)}, u32[]{:S(2)}) collective-permute-start(bf16[8,256]{1,0:T(8,128)(2,1)S(1)} %collective-permute-done.4), channel_id=1, source_target_pairs={{0,1},{1,2},{2,3},{3,4},{4,5},{5,6},{6,7},{7,0},{8,9},{9,10},{10,1... | collective-permute-start | bytes 12296 | tf_op jit(solution)/shard_map/ppermute | solution.py:16
  116.0 4.8 %collective-permute-start.6 = (bf16[8,256]{1,0:T(8,128)(2,1)S(1)}, bf16[8,256]{1,0:T(8,128)(2,1)S(1)}, u32[]{:S(2)}, u32[]{:S(2)}) collective-permute-start(bf16[8,256]{1,0:T(8,128)(2,1)S(1)} %collective-permute-done.5), channel_id=1, source_target_pairs={{0,1},{1,2},{2,3},{3,4},{4,5},{5,6},{6,7},{7,0},{8,9},{9,10},{10,1... | collective-permute-start | bytes 12296 | tf_op jit(solution)/shard_map/ppermute | solution.py:16
Sparse Core Ops, SparseCore 0:
  18.7 37.6 all-reduce.7
  80.0 6.2 reduce-scatter.2
  127.9 28.8 reduce-scatter.4
